TPU v7x, 32 devices: a whole 2x2x4 slice. The times are simulated.
32 devices in a mesh: sp: 8 (over z, y), dp: 4 (over x, core).
Axes of the slice: x: 2, y: 2, z: 4, core: 2. Of those that a mesh axis runs over, the one named last changes fastest.
Arguments:
- tokens: bfloat16 [4, 4096, 2048], P('dp', 'sp'), may hold values from -6 to 6
- norm_gain: float32 [2048], replicated, may hold values from 0.1 to 1.9
- w_query: bfloat16 [2048, 1024], P(('sp', 'dp')), may hold values from -0.125 to 0.125
- w_key: bfloat16 [2048, 1024], P(('sp', 'dp')), may hold values from -0.125 to 0.125
- w_value: bfloat16 [2048, 2048], P(('sp', 'dp')), may hold values from -0.125 to 0.125
- w_out: bfloat16 [2048, 2048], P(('sp', 'dp')), may hold values from -0.125 to 0.125
- decay_rate: float32 [4, 8, 32], P('dp'), may hold values from 1.2207031e-05 to 0.08, as said below
Outputs:
- layer_out: bfloat16 [4, 4096, 2048], P('dp', 'sp')
Inputs may be any that keep to these rules, and one draw needn't show every extreme that they name: `decay_rate`: one rate for each sequence, head and block of 128 positions.
All inputs are finite; a program needn't handle non-finite values.
Results may differ from a plain program's by a relative error of at most 0.02.
Values may be sent and summed in bfloat16 or wider, within the bound.
A program may use at most 128 MiB of HBM per device.

v0:
```python
import jax
import jax.numpy as jnp
from jax import lax
from jax.sharding import PartitionSpec as P

HEADS = 8
DK = 128
DV = 256
GROUP_W = 128
BLOCK = 128


EPS_RMS = 1e-06
EPS_GROUP = 0.01
ROPE_BASE = 10000.0


def carried_in(x, axis, join, neutral):
    place = lax.axis_index(axis)
    gathered = jax.tree.map(
        lambda a, kind: lax.all_gather(a.astype(kind), axis), x, (jnp.bfloat16, jnp.bfloat16)
    )
    state = jax.tree.map(lambda a, e: jnp.zeros_like(a) + jnp.asarray(e, a.dtype), x, neutral)

    def one(lap, state):
        return join(
            state,
            jax.tree.map(
                lambda a, own: lax.dynamic_index_in_dim(a, lap, 0, False).astype(own.dtype),
                gathered,
                x,
            ),
        )

    return lax.fori_loop(0, place, one, state)


def rms_scaled(token_rows, norm_gain):
    widened = token_rows.astype(jnp.float32)
    inv_norm = lax.rsqrt(jnp.mean(widened * widened, axis=-1, keepdims=True) + EPS_RMS)
    return (widened * inv_norm * norm_gain).astype(jnp.bfloat16)


def rope_tables(length, head_depth, first_pos):
    half_depth = head_depth // 2
    inverse = ROPE_BASE ** (-(jnp.arange(half_depth, dtype=jnp.float32) / (half_depth - 1)))
    places = first_pos.astype(jnp.float32) + jnp.arange(length, dtype=jnp.float32)
    angles = places[:, None] * inverse[None, :]
    return (jnp.cos(angles), jnp.sin(angles))


def rotate(stacked, cosine_table, sine_table):
    paired = stacked.reshape(stacked.shape[0], stacked.shape[1], -1, 2)
    first_part = paired[..., 0]
    second_part = paired[..., 1]
    cos_rows = cosine_table[:, None, :]
    sin_rows = sine_table[:, None, :]
    turned = jnp.stack(
        [
            first_part * cos_rows - second_part * sin_rows,
            second_part * cos_rows + first_part * sin_rows,
        ],
        axis=-1,
    )
    return turned.reshape(stacked.shape)


def combine_pairs(earlier, later):
    return (earlier[0] * later[0], later[0][..., None, None] * earlier[1] + later[1])


def from_earlier(last_decay, last_state):
    _, incoming = carried_in(
        (last_decay, last_state),
        "sp",
        combine_pairs,
        (jnp.ones_like(last_decay), jnp.zeros_like(last_state)),
    )
    return incoming


def retain(queries, keys_in, values_in, decay_rows, carry_in):
    length, groups, head_depth = queries.shape
    blocks = length // BLOCK

    def by_block(stacked):
        return stacked.reshape(blocks, BLOCK, groups, stacked.shape[-1]).transpose(2, 0, 1, 3)

    query_blocks = by_block(queries)
    key_blocks = by_block(keys_in)
    value_blocks = by_block(values_in)
    offsets = jnp.arange(BLOCK, dtype=jnp.float32)
    distance = offsets[:, None] - offsets[None, :]
    within = jnp.where(
        distance >= 0.0, jnp.exp(-decay_rows[:, :, None, None] * jnp.maximum(distance, 0.0)), 0.0
    )
    scores = jnp.einsum(
        "gncd,gnmd->gncm", query_blocks, key_blocks, preferred_element_type=jnp.float32
    )
    weighted = (scores * within).astype(jnp.bfloat16)
    inner_sum = jnp.einsum(
        "gncm,gnme->gnce", weighted, value_blocks, preferred_element_type=jnp.float32
    )
    to_end = jnp.exp(-decay_rows[:, :, None] * (BLOCK - 1.0 - offsets))
    key_scaled = (key_blocks.astype(jnp.float32) * to_end[..., None]).astype(jnp.bfloat16)
    local_state = jnp.einsum(
        "gncd,gnce->gnde", key_scaled, value_blocks, preferred_element_type=jnp.float32
    )
    carried = jnp.exp(-decay_rows * BLOCK)
    cum_decay, cum_state = lax.associative_scan(combine_pairs, (carried, local_state), axis=1)
    incoming = carry_in(cum_decay[:, -1], cum_state[:, -1])
    before_local = jnp.concatenate([jnp.zeros_like(cum_state[:, :1]), cum_state[:, :-1]], axis=1)
    decay_before = jnp.concatenate([jnp.ones_like(cum_decay[:, :1]), cum_decay[:, :-1]], axis=1)
    before = before_local + decay_before[..., None, None] * incoming[:, None]
    from_start = jnp.exp(-decay_rows[:, :, None] * (offsets + 1.0))
    cross_term = jnp.einsum(
        "gncd,gnde->gnce",
        query_blocks.astype(jnp.float32) * from_start[..., None],
        before,
        precision=lax.Precision.HIGHEST,
    )
    mixed = inner_sum + cross_term
    return mixed.transpose(1, 2, 0, 3).reshape(length, groups, values_in.shape[-1])


def row_adder(left):

    def add_rows(running_sum, weight_piece, row_start):
        return jnp.dot(left, weight_piece, preferred_element_type=jnp.float32)

    return add_rows


def body(tokens, norm_gain, w_query, w_key, w_value, w_out, decay_rate):
    token_rows = tokens[0]
    local_count = token_rows.shape[0]
    normed_in = rms_scaled(token_rows, norm_gain)
    add_rows = row_adder(normed_in)
    query_empty = jnp.zeros((local_count, w_query.shape[1]), jnp.float32)
    value_empty = jnp.zeros((local_count, w_value.shape[1]), jnp.float32)
    out_empty = jnp.zeros((local_count, w_out.shape[1]), jnp.float32)
    row_start = jnp.int32(0)
    query_sum = add_rows(
        query_empty, lax.all_gather(w_query, ("sp", "dp"), axis=0, tiled=True), row_start
    )
    key_sum = add_rows(
        query_empty, lax.all_gather(w_key, ("sp", "dp"), axis=0, tiled=True), row_start
    )
    value_sum = add_rows(
        value_empty, lax.all_gather(w_value, ("sp", "dp"), axis=0, tiled=True), row_start
    )
    shard_index = lax.axis_index("sp")
    cosine_table, sine_table = rope_tables(local_count, DK, shard_index * local_count)
    query_rot = rotate(
        query_sum.astype(jnp.bfloat16).astype(jnp.float32).reshape(local_count, HEADS, DK),
        cosine_table,
        sine_table,
    ).astype(jnp.bfloat16)
    key_rot = (
        rotate(
            key_sum.astype(jnp.bfloat16).astype(jnp.float32).reshape(local_count, HEADS, DK),
            cosine_table,
            sine_table,
        )
        * DK ** (-0.5)
    ).astype(jnp.bfloat16)
    value_groups = value_sum.astype(jnp.bfloat16).reshape(local_count, 2 * HEADS, GROUP_W)
    blocks_here = local_count // BLOCK
    own_rates = lax.dynamic_slice_in_dim(decay_rate[0], shard_index * blocks_here, blocks_here, 1)
    mixed = retain(
        jnp.concatenate([query_rot, query_rot], axis=1),
        jnp.concatenate([key_rot, key_rot], axis=1),
        value_groups,
        jnp.concatenate([own_rates, own_rates], axis=0),
        from_earlier,
    )
    halves = mixed.reshape(local_count, 2, HEADS, GROUP_W)
    mean_part = jnp.sum(halves, axis=(1, 3), keepdims=True) / DV
    square_part = jnp.sum(halves * halves, axis=(1, 3), keepdims=True) / DV
    retained = (
        ((halves - mean_part) * lax.rsqrt(square_part - mean_part * mean_part + EPS_GROUP))
        .astype(jnp.bfloat16)
        .reshape(local_count, -1)
    )
    result = row_adder(retained)(
        out_empty, lax.all_gather(w_out, ("sp", "dp"), axis=0, tiled=True), jnp.int32(0)
    )
    return result.astype(jnp.bfloat16)[None]


def solution(mesh):
    in_specs = (
        P("dp", "sp", None),
        P(),
        P(("sp", "dp"), None),
        P(("sp", "dp"), None),
        P(("sp", "dp"), None),
        P(("sp", "dp"), None),
        P("dp", None, None),
    )
    out_specs = P("dp", "sp", None)
    return jax.shard_map(body, mesh=mesh, in_specs=in_specs, out_specs=out_specs, check_vma=False)
```

profile of v0, /device:TPU:28, one launch (start us, length us, event | category | flops | bytes accessed | tf_op | source)
XLA Modules:
  0.0 422.8 jit_solution(6517133512220960198)
XLA Ops:
  9.3 2.1 fusion
  12.1 59.6 %all-gather.8.cloned.1.call-done = bf16[2048,1024]{1,0:T(8,128)(2,1)} async-done(((bf16[64,1024]{1,0:T(8,128)(2,1)}), bf16[2048,1024]{1,0:T(8,128)(2,1)}) %all-gather.8.cloned.1.call-update) | async-done | bytes 4194320 | tf_op jit(solution)/shard_map/all_gather | solution.py:144
  71.7 6.5 %fusion.23 = f32[512,1024]{1,0:T(8,128)} fusion(bf16[2048,1024]{1,0:T(8,128)(2,1)} %all-gather.8.cloned.1.call-done, bf16[1,512,2048]{2,1,0:T(8,128)(2,1)} %param.9, f32[2048]{0:T(1024)} %param.10, f32[512]{0:T(512)S(1)} %add_rsqrt_fusion.1), kind=kOutput, calls=%fused_computation.45 | convolution fusion | flops 2152726528 | bytes 8398848 | tf_op jit(solution)/shard_map/dot_general | solution.py:129
  78.2 1.9 copy.52
  80.1 2.2 reshape.213
  82.4 52.7 %all-gather.10.cloned.1.call-done = bf16[2048,1024]{1,0:T(8,128)(2,1)} async-done(((bf16[64,1024]{1,0:T(8,128)(2,1)}), bf16[2048,1024]{1,0:T(8,128)(2,1)}) %all-gather.10.cloned.1.call-update) | async-done | bytes 4194320 | tf_op jit(solution)/shard_map/all_gather | solution.py:147
  135.1 6.5 %fusion.22 = f32[512,1024]{1,0:T(8,128)} fusion(bf16[2048,1024]{1,0:T(8,128)(2,1)} %all-gather.10.cloned.1.call-done, bf16[1,512,2048]{2,1,0:T(8,128)(2,1)} %param.9, f32[2048]{0:T(1024)S(1)} %copy-done.9, f32[512]{0:T(512)S(1)} %add_rsqrt_fusion.1), kind=kOutput, calls=%fused_computation.43 | convolution fusion | flops 2152726528 | bytes 8398848 | tf_op jit(solution)/shard_map/dot_general | solution.py:129
  141.6 1.9 copy.58
  143.5 2.3 reshape.214
  145.8 8.2 %fusion.41 = (f32[512,8,64,1]{0,3,2,1:T(1,128)S(1)}, f32[512,8,64,1]{0,3,2,1:T(1,128)S(1)}, f32[512,8,64,1]{0,3,2,1:T(1,128)S(1)}, f32[512,8,64,1]{0,3,2,1:T(1,128)S(1)}) fusion(f32[512,8,64,2]{0,3,2,1:T(2,128)} %reshape.213, f32[512,8,64,2]{0,3,2,1:T(2,128)} %reshape.214), kind=kLoop, calls=%fused_computation.89 | loop fusion | bytes 8388608 | tf_op jit(solution)/shard_map/slice | solution.py:54
  154.0 1.7 subtract_convert_fusion
  157.9 55.7 %all-gather.12.cloned.1.call-done = bf16[2048,2048]{1,0:T(8,128)(2,1)} async-done(((bf16[64,2048]{1,0:T(8,128)(2,1)}), bf16[2048,2048]{1,0:T(8,128)(2,1)}) %all-gather.12.cloned.1.call-update) | async-done | bytes 8388624 | tf_op jit(solution)/shard_map/all_gather | solution.py:150
  213.6 8.6 %fusion.21 = bf16[64,8,16,128]{3,1,2,0:T(8,128)(2,1)S(1)} fusion(bf16[2048,2048]{1,0:T(8,128)(2,1)} %all-gather.12.cloned.1.call-done, bf16[1,512,2048]{2,1,0:T(8,128)(2,1)} %param.9, f32[2048]{0:T(1024)S(1)} %copy-done.9, f32[512]{0:T(512)S(1)} %add_rsqrt_fusion.1), kind=kOutput, calls=%fused_computation.41 | convolution fusion | flops 4300210176 | bytes 12593152 | tf_op jit(solution)/shard_map/dot_general | solution.py:129
  222.8 3.3 fusion.11
  226.4 1.7 copy-done.2
  230.8 18.2 %pad.111 = f32[16,3,128,128]{3,2,1,0:T(8,128)} pad(f32[16,2,128,128]{3,2,1,0:T(8,128)} %pad_add_fusion, f32[]{:T(128)} %constant.23.clone.1), padding=0_0_0x0_0_1x0_0_0x0_0_0 | pad | bytes 5242884
  249.0 2.1 add_convert_fusion
  253.3 17.2 %all-reduce.10 = bf16[128]{0:T(256)(128)(2,1)S(1)} all-reduce(bf16[128]{0:T(256)(128)(2,1)S(1)} %dynamic-update-slice), channel_id=2, replica_groups=mesh['sp'=8,'dp'=4] {'sp'}, use_global_device_ids=true, to_apply=%add.10 | all-reduce | flops 128 | bytes 512
  272.2 1.6 copy.55
  273.8 2.2 convert_element_type.101
  275.9 2.7 copy.56
  278.6 18.5 %pad.31 = f32[16,4,128,128]{3,2,1,0:T(8,128)} pad(f32[16,2,128,128]{3,2,1,0:T(8,128)} %pad_add_fusion, f32[]{:T(128)} %constant.23.clone.1), padding=0_0_0x1_0_1x0_0_0x0_0_0 | pad | bytes 6291460 | tf_op jit(solution)/shard_map/pad | solution.py:110
  297.1 2.1 fusion.40
  300.7 18.5 %pad.30 = f32[16,4,128,128]{3,2,1,0:T(8,128)} pad(f32[16,2,128,128]{3,2,1,0:T(8,128)} %pad_maximum_fusion, f32[]{:T(128)} %constant.23.clone.1), padding=0_0_0x0_1_1x0_0_0x0_0_0 | pad | bytes 6291460 | tf_op jit(solution)/shard_map/pad | solution.py:110
  319.2 1.7 bitcast_bitcast_fusion
  322.1 4.4 %slice_add_fusion = f32[16,3,128,128]{3,2,1,0:T(8,128)} fusion(f32[16,4,128,128]{3,2,1,0:T(8,128)S(1)} %copy-done.3, f32[16,4,128,128]{3,2,1,0:T(8,128)} %pad.30), kind=kLoop, calls=%fused_computation.20 | loop fusion | flops 786432 | bytes 9437184 | tf_op jit(solution)/shard_map/add | solution.py:110
  326.7 9.5 %while.12 = (s32[]{:T(128)}, f32[16,128,128]{2,1,0:T(8,128)S(1)}, s32[]{:T(128)}, bf16[8,16]{1,0:T(8,128)(2,1)S(1)}, bf16[8,16,128,128]{3,2,1,0:T(8,128)(2,1)}, /*index=5*/s32[]{:T(128)}, s32[]{:T(128)}, s32[]{:T(128)}) while((s32[]{:T(128)}, f32[16,128,128]{2,1,0:T(8,128)S(1)}, s32[]{:T(128)}, bf16[8,16]{1,0:T(8,128)(2,1)S(1)}, ...), condition=%wide.region_2.3_spmd, body=%wide.region_1.2_spmd.sunk | while | flops 786453 | bytes 2621727 | solution.py:35
  336.2 11.1 %fusion.4 = f32[16,4,128,128]{2,3,1,0:T(8,128)} fusion(f32[16,3,128,128]{3,2,1,0:T(8,128)} %slice_add_fusion, f32[16,128,128]{2,1,0:T(8,128)S(1)} %get-tuple-element.49, f32[16,4]{1,0:T(8,128)S(1)} %concatenate.40.clone, f32[16,4,128]{2,1,0:T(4,128)S(1)} %get-tuple-element.80, bf16[4,128,8,128]{3,1,0,2:T(8,128)(2,1)S(1)} %copy-done.8), kind=kOutput, calls=%fused_computation.12 | convolution fusion | flops 1615855616 | bytes 9470208 | tf_op jit(solution)/shard_map/gncd,gnde->gnce/dot_general | solution.py:116
  347.3 6.9 %fusion.38 = (f32[4,128,16]{1,0,2:T(4,128)S(1)}, f32[4,128,16]{1,0,2:T(4,128)S(1)}, f32[4,128,16,128]{1,3,0,2:T(8,128)}) fusion(f32[16,4,128,128]{2,3,1,0:T(8,128)} %fusion.4, bf16[16,4,128,128]{3,0,2,1:T(8,128)(2,1)} %bitcast_bitcast_fusion, f32[128,128]{1,0:T(8,128)S(1)} %fusion.27, f32[16,4]{1,0:T(8,128)S(1)} %copy.65, pred[128,128]{1,0:T(8,128)(4,1)S(1)} %fusion.28, ...), kind=kOutput, calls=%fused_computation.86 | convolution fusion | flops 547340288 | bytes 12730624 | tf_op jit(solution)/shard_map/gncm,gnme->gnce/dot_general | solution.py:101
  354.6 5.5 %copy.73 = f32[4,128,16,128]{3,2,1,0:T(8,128)} copy(f32[4,128,16,128]{1,3,0,2:T(8,128)} %get-tuple-element.92) | data formatting | bytes 8388608 | tf_op jit(solution)/shard_map/add | solution.py:122
  360.0 41.2 %all-gather.14.cloned.1.call-done = bf16[2048,2048]{1,0:T(8,128)(2,1)} async-done(((bf16[64,2048]{1,0:T(8,128)(2,1)}), bf16[2048,2048]{1,0:T(8,128)(2,1)}) %all-gather.14.cloned.1.call-update) | async-done | bytes 8388624 | tf_op jit(solution)/shard_map/all_gather | solution.py:186
  404.1 12.2 %fusion.10 = bf16[1,512,2048]{2,1,0:T(8,128)(2,1)} fusion(bf16[2048,2048]{1,0:T(8,128)(2,1)} %all-gather.14.cloned.1.call-done, f32[64,8,16,128]{3,2,1,0:T(8,128)S(1)} %bitcast.105, f32[64,8,16,128]{3,2,1,0:T(8,128)S(1)} %bitcast.104, f32[64,8,16,128]{3,2,1,0:T(8,128)S(1)} %bitcast.103), kind=kOutput, calls=%fused_computation.23 | convolution fusion | flops 4299161600 | bytes 23068672 | tf_op jit(solution)/shard_map/dot_general | solution.py:129
  (96 shorter events, 27.4 us)
Async XLA Ops:
  6.5 2.3 copy-start
  6.5 65.1 %all-gather.8.cloned.1.call-start = ((), (), s32[]{:S(2)}) async-start(), calls=%async_computation | async-start | bytes 4325376 | tf_op jit(solution)/shard_map/all_gather | solution.py:144
  7.3 127.8 %all-gather.10.cloned.1.call-start = ((), (), s32[]{:S(2)}) async-start(), calls=%async_computation.1 | async-start | bytes 4325376 | tf_op jit(solution)/shard_map/all_gather | solution.py:147
  8.0 205.6 %all-gather.12.cloned.1.call-start = ((), (), s32[]{:S(2)}) async-start(), calls=%async_computation.2 | async-start | bytes 8650752 | tf_op jit(solution)/shard_map/all_gather | solution.py:150
  8.7 317.8 %all-gather.16.cloned.1.call-start = ((), (), s32[]{:S(2)}) async-start(), calls=%async_computation.4 | async-start | bytes 4718592 | tf_op jit(solution)/shard_map/all_gather | solution.py:21
  78.2 56.9 %copy-start.9 = (f32[2048]{0:T(1024)S(1)}, f32[2048]{0:T(1024)}, u32[]{:S(2)}) copy-start(f32[2048]{0:T(1024)} %param.10) | copy-start | bytes 24580
  157.9 64.9 %copy-start.5 = (bf16[4,128,8,128]{3,1,0,2:T(8,128)(2,1)}, bf16[4,128,8,128]{3,1,0,2:T(8,128)(2,1)S(1)}, u32[]{:S(2)}) copy-start(bf16[4,128,8,128]{3,1,0,2:T(8,128)(2,1)S(1)} %copy.62) | copy-start | bytes 3145732
  226.1 1.9 copy-start.2
  228.3 1.0 copy-start.4
  230.8 21.0 %copy-start.10 = (u32[32]{0:T(128)S(1)}, u32[32]{0:T(128)}, u32[]{:S(2)}) copy-start(u32[32]{0:T(128)} %constant.85) | copy-start | bytes 388
  251.1 150.1 %all-gather.14.cloned.1.call-start = ((), (), s32[]{:S(2)}) async-start(), calls=%async_computation.3 | async-start | bytes 8650752 | tf_op jit(solution)/shard_map/all_gather | solution.py:186
  319.2 2.9 copy-start.3
  326.7 9.5 %copy-start.8 = (bf16[4,128,8,128]{3,1,0,2:T(8,128)(2,1)S(1)}, bf16[4,128,8,128]{3,1,0,2:T(8,128)(2,1)}, u32[]{:S(2)}) copy-start(bf16[4,128,8,128]{3,1,0,2:T(8,128)(2,1)} %copy.56) | copy-start | bytes 3145732
  336.2 11.1 %copy-start.6 = (bf16[4,128,8,128]{3,1,0,2:T(8,128)(2,1)S(1)}, bf16[4,128,8,128]{3,1,0,2:T(8,128)(2,1)}, u32[]{:S(2)}) copy-start(bf16[4,128,8,128]{3,1,0,2:T(8,128)(2,1)} %copy-done.5) | copy-start | bytes 3145732
  401.9 2.2 copy-start.7
  404.0 12.2 %copy-start.1 = (f32[1,8,32]{2,1,0:T(8,128)S(1)}, f32[1,8,32]{2,1,0:T(8,128)}, u32[]{:S(2)}) copy-start(f32[1,8,32]{2,1,0:T(8,128)} %param.15) | copy-start | bytes 3076
Sparse Core Ops, SparseCore 0:
  10.2 61.4 all-gather.7
  74.5 60.4 all-gather.9
  137.9 75.6 all-gather.11
  251.2 70.6 all-gather.15
  324.6 76.5 all-gather.13
where the time goes:
time: 430 us; the launch traced here: 423 us
  waiting for transfers between devices  212 us (49%)
  local copies, waits for them, and re-layouts  96.4 us (22%)
  matrix products  55.1 us (13%)
  other arithmetic  27.6 us (6%)
  blocking collectives  17.2 us (4%)
  between operations  14.2 us (3%)
    all_gather x1, waiting for transfers between devices, body(): lax.all_gather(w_query, ('sp', 'dp'), axis=0, tiled=True)  59.6 us
    all_gather x1, waiting for transfers between devices, body(): lax.all_gather(w_value, ('sp', 'dp'), axis=0, tiled=True)  55.7 us
    all_gather x1, waiting for transfers between devices, body(): lax.all_gather(w_key, ('sp', 'dp'), axis=0, tiled=True)  52.7 us
    all_gather x1, waiting for transfers between devices, body(): lax.all_gather(w_out, ('sp', 'dp'), axis=0, tiled=True)  41.2 us
    pad x4, local copies, waits for them, and re-layouts, retain(): lax.associative_scan(combine_pairs, (carried, local_state), axis=1)  37.1 us
    dot_general x4, matrix products, add_rows(): return jnp.dot(left, weight_piece, preferred_element_type=jnp.float32)  33.8 us
    unnamed x29, local copies, waits for them, and re-layouts  25.3 us
    unnamed x1, blocking collectives  17.2 us
  transfers between devices with their start and end apart: 5, of which 4 were waited for; matrix products, arithmetic and copies ran while one was open for 30% of the time, Pallas kernels for 0%

commit v1 on v0

--- a/solution.py
+++ b/solution.py
@@ -1,6 +1,9 @@
 import jax
 import jax.numpy as jnp
+import functools
 from jax import lax
+from jax.experimental import pallas as pl
+from jax.experimental.pallas import tpu as pltpu
 from jax.sharding import PartitionSpec as P
 
 HEADS = 8
@@ -13,6 +16,209 @@
 EPS_RMS = 1e-06
 EPS_GROUP = 0.01
 ROPE_BASE = 10000.0
+MESH = pl.DeviceIdType.MESH
+
+LINE_ORDERS = ((0, 1, 2), (0, 2, 1), (1, 2, 0), (2, 1, 0))
+SHARE = (3, 3, 1, 1)
+WAVES = 3
+SKEW = 2
+
+
+def chip_grid(mesh_shape):
+    sp, dp = mesh_shape["sp"], mesh_shape["dp"]
+    y_size = max(k for k in range(1, sp + 1) if sp % k == 0 and k * k <= sp)
+    return (sp // y_size, y_size, dp // 2)
+
+
+def project_kernel(grid, x_ref, gain_ref, own_ref, proj_ref, out_w_ref, g_ref, normed_ref,
+                   own_sem, out_sem, recv_sem, pair_recv, send_sem, pair_send):
+    z_size, y_size, x_size = grid
+    chips = z_size * y_size * x_size
+    rows = own_ref.shape[0]
+    width = own_ref.shape[1] // WAVES
+    sp_at = lax.axis_index("sp")
+    dp_at = lax.axis_index("dp")
+    core = lax.rem(dp_at, 2)
+    here = (sp_at // y_size, lax.rem(sp_at, y_size), dp_at // 2)
+
+    def device(place, core_at):
+        return {"sp": place[0] * y_size + place[1], "dp": place[2] * 2 + core_at}
+
+    def moved(dim, sign):
+        return tuple(at + sign if k == dim else at for k, at in enumerate(here))
+
+    def in_range(dim, sign):
+        return here[dim] + 1 < grid[dim] if sign > 0 else here[dim] > 0
+
+    ways = [(dim, sign) for dim in range(3) if grid[dim] > 1 for sign in (1, -1)]
+    barrier = pltpu.get_barrier_semaphore()
+    pl.semaphore_signal(barrier, inc=1, device_id=device(here, 1 - core), device_id_type=MESH)
+    peers = 1
+    for dim, sign in ways:
+        @pl.when(in_range(dim, sign))
+        def _(dim=dim, sign=sign):
+            pl.semaphore_signal(
+                barrier, inc=1, device_id=device(moved(dim, sign), core), device_id_type=MESH
+            )
+    for dim, sign in ways:
+        peers = peers + jnp.where(in_range(dim, sign), 1, 0)
+    pl.semaphore_wait(barrier, peers)
+
+    me = (here[0] * y_size + here[1]) * x_size + here[2]
+
+    def row_at(chip, core_at):
+        return pl.multiple_of((chip * 2 + core_at) * rows, rows)
+
+    own = pltpu.make_async_copy(own_ref, g_ref.at[pl.ds(row_at(me, core), rows), :], own_sem)
+    own.start()
+    own.wait()
+    unit = width // sum(SHARE)
+
+    def piece(w, q, start, size, core_at):
+        first = pl.multiple_of(w * width + start, 128)
+        return g_ref.at[pl.ds(row_at(q, core_at), rows), pl.ds(first, size)]
+
+    def copies(w, q):
+        found = []
+        gone = (
+            here[0] - q // (y_size * x_size),
+            here[1] - lax.rem(q // x_size, y_size),
+            here[2] - lax.rem(q, x_size),
+        )
+        pair = pltpu.make_async_remote_copy(
+            src_ref=piece(w, q, 0, width, core), dst_ref=piece(w, q, 0, width, core),
+            send_sem=pair_send.at[q], recv_sem=pair_recv.at[w, q],
+            device_id=device(here, 1 - core), device_id_type=MESH,
+        )
+        start = 0
+        for kind, order in enumerate(LINE_ORDERS):
+            size = SHARE[kind] * unit
+            for spot, (dim, sign) in enumerate(ways):
+                keep = in_range(dim, sign) & (gone[dim] * sign >= 0)
+                for later in order[order.index(dim) + 1:]:
+                    keep = keep & (gone[later] == 0)
+                ref = piece(w, q, start, size, core)
+                found.append((keep, pltpu.make_async_remote_copy(
+                    src_ref=ref, dst_ref=ref,
+                    send_sem=send_sem.at[q, kind * len(ways) + spot],
+                    recv_sem=recv_sem.at[w, q],
+                    device_id=device(moved(dim, sign), core), device_id_type=MESH,
+                )))
+            start += size
+        distance = abs(gone[0]) + abs(gone[1]) + abs(gone[2])
+        return distance, pair, found
+
+    def forward(w, r):
+        def one(q, _):
+            distance, pair, found = copies(w, q)
+
+            @pl.when(distance == r)
+            def _():
+                @pl.when(r > 0)
+                def _():
+                    full = piece(w, q, 0, width, core)
+                    pltpu.make_async_copy(full, full, recv_sem.at[w, q]).wait()
+                for keep, copy in found:
+                    @pl.when(keep)
+                    def _(copy=copy):
+                        copy.start()
+                pair.start()
+            return 0
+        lax.fori_loop(0, chips, one, 0)
+
+    def run(first, last):
+        def at(t, _):
+            def wave(w, _):
+                forward(w, t - SKEW * w)
+                return 0
+            return lax.fori_loop(0, WAVES, wave, 0)
+        lax.fori_loop(first, last, at, 0)
+
+    def pair_done(w):
+        def one(q, _):
+            full = piece(w, q, 0, width, 1 - core)
+            pltpu.make_async_copy(full, full, pair_recv.at[w, q]).wait()
+            return 0
+        lax.fori_loop(0, chips, one, 0)
+
+    count = x_ref.shape[0]
+    tile = 256
+
+    def project(w):
+        def one(n, _):
+            columns = pl.ds(pl.multiple_of(w * width + n * tile, tile), tile)
+            proj_ref[:, columns] = jnp.dot(
+                normed_ref[...], g_ref[:, columns], preferred_element_type=jnp.float32
+            ).astype(jnp.bfloat16)
+            return 0
+        lax.fori_loop(0, width // tile, one, 0)
+
+    last_round = sum(size - 1 for size in grid)
+    run(0, 1)
+
+    def norm(n, _):
+        at = pl.ds(pl.multiple_of(n * 64, 64), 64)
+        wide = x_ref[at, :].astype(jnp.float32)
+        scale = lax.rsqrt(jnp.mean(wide * wide, axis=-1, keepdims=True) + EPS_RMS)
+        normed_ref[at, :] = (wide * scale * gain_ref[...]).astype(jnp.bfloat16)
+        return 0
+    lax.fori_loop(0, count // 64, norm, 0)
+
+    run(1, last_round + 1)
+    pair_done(0)
+    project(0)
+    run(last_round + 1, last_round + SKEW + 1)
+    pair_done(1)
+    project(1)
+    run(last_round + SKEW + 1, last_round + 2 * SKEW + 1)
+    pair_done(2)
+    leave = pltpu.make_async_copy(g_ref.at[:, pl.ds(2 * width, width)], out_w_ref, out_sem)
+    leave.start()
+
+    def drain(q, _):
+        _, _, found = copies(0, q)
+        for slot, (keep, _) in enumerate(found):
+            @pl.when(keep)
+            def _(slot=slot):
+                sent = piece(0, q, 0, WAVES * SHARE[slot // len(ways)] * unit, core)
+                pltpu.make_async_copy(sent, sent, send_sem.at[q, slot]).wait()
+        sent = piece(0, q, 0, WAVES * width, core)
+        pltpu.make_async_copy(sent, sent, pair_send.at[q]).wait()
+        return 0
+    lax.fori_loop(0, chips, drain, 0)
+    leave.wait()
+
+
+def projected(grid, token_rows, norm_gain, own_rows):
+    count, depth = token_rows.shape
+    rows, columns = own_rows.shape
+    width = columns // WAVES
+    chips = grid[0] * grid[1] * grid[2]
+    ways = 2 * sum(size > 1 for size in grid)
+    vmem = pl.BlockSpec(memory_space=pltpu.VMEM)
+    hbm = pl.BlockSpec(memory_space=pl.ANY)
+    return pl.pallas_call(
+        functools.partial(project_kernel, grid),
+        out_shape=(
+            jax.ShapeDtypeStruct((count, 2 * width), jnp.bfloat16),
+            jax.ShapeDtypeStruct((depth, width), jnp.bfloat16),
+        ),
+        in_specs=[vmem, vmem, hbm],
+        out_specs=(vmem, hbm),
+        scratch_shapes=[
+            pltpu.VMEM((depth, columns), jnp.bfloat16),
+            pltpu.VMEM((count, depth), jnp.bfloat16),
+            pltpu.SemaphoreType.DMA,
+            pltpu.SemaphoreType.DMA,
+            pltpu.SemaphoreType.DMA((WAVES, chips)),
+            pltpu.SemaphoreType.DMA((WAVES, chips)),
+            pltpu.SemaphoreType.DMA((chips, 4 * ways)),
+            pltpu.SemaphoreType.DMA((chips,)),
+        ],
+        compiler_params=pltpu.CompilerParams(
+            collective_id=0, has_side_effects=True, vmem_limit_bytes=60 * 1024 * 1024
+        ),
+    )(token_rows, norm_gain[None, :], own_rows)
 
 
 def carried_in(x, axis, join, neutral):
@@ -33,12 +239,6 @@
         )
 
     return lax.fori_loop(0, place, one, state)
-
-
-def rms_scaled(token_rows, norm_gain):
-    widened = token_rows.astype(jnp.float32)
-    inv_norm = lax.rsqrt(jnp.mean(widened * widened, axis=-1, keepdims=True) + EPS_RMS)
-    return (widened * inv_norm * norm_gain).astype(jnp.bfloat16)
 
 
 def rope_tables(length, head_depth, first_pos):
@@ -123,32 +323,16 @@
     return mixed.transpose(1, 2, 0, 3).reshape(length, groups, values_in.shape[-1])
 
 
-def row_adder(left):
-
-    def add_rows(running_sum, weight_piece, row_start):
-        return jnp.dot(left, weight_piece, preferred_element_type=jnp.float32)
-
-    return add_rows
-
-
-def body(tokens, norm_gain, w_query, w_key, w_value, w_out, decay_rate):
+def body(grid, tokens, norm_gain, w_query, w_key, w_value, w_out, decay_rate):
     token_rows = tokens[0]
     local_count = token_rows.shape[0]
-    normed_in = rms_scaled(token_rows, norm_gain)
-    add_rows = row_adder(normed_in)
-    query_empty = jnp.zeros((local_count, w_query.shape[1]), jnp.float32)
-    value_empty = jnp.zeros((local_count, w_value.shape[1]), jnp.float32)
-    out_empty = jnp.zeros((local_count, w_out.shape[1]), jnp.float32)
-    row_start = jnp.int32(0)
-    query_sum = add_rows(
-        query_empty, lax.all_gather(w_query, ("sp", "dp"), axis=0, tiled=True), row_start
-    )
-    key_sum = add_rows(
-        query_empty, lax.all_gather(w_key, ("sp", "dp"), axis=0, tiled=True), row_start
-    )
-    value_sum = add_rows(
-        value_empty, lax.all_gather(w_value, ("sp", "dp"), axis=0, tiled=True), row_start
-    )
+    own_rows = jnp.concatenate([w_key, w_value, w_query, w_out], axis=1)
+    proj, out_rows = projected(grid, token_rows, norm_gain, own_rows)
+    key_end = w_key.shape[1]
+    value_end = key_end + w_value.shape[1]
+    key_sum = proj[:, :key_end]
+    value_sum = proj[:, key_end:value_end]
+    query_sum = proj[:, value_end:]
     shard_index = lax.axis_index("sp")
     cosine_table, sine_table = rope_tables(local_count, DK, shard_index * local_count)
     query_rot = rotate(
@@ -182,9 +366,7 @@
         .astype(jnp.bfloat16)
         .reshape(local_count, -1)
     )
-    result = row_adder(retained)(
-        out_empty, lax.all_gather(w_out, ("sp", "dp"), axis=0, tiled=True), jnp.int32(0)
-    )
+    result = jnp.dot(retained, out_rows, preferred_element_type=jnp.float32)
     return result.astype(jnp.bfloat16)[None]
 
 
@@ -199,4 +381,4 @@
         P("dp", None, None),
     )
     out_specs = P("dp", "sp", None)
-    return jax.shard_map(body, mesh=mesh, in_specs=in_specs, out_specs=out_specs, check_vma=False)
+    return jax.shard_map(functools.partial(body, chip_grid(mesh.shape)), mesh=mesh, in_specs=in_specs, out_specs=out_specs, check_vma=False)

time: 430 us -> 308 us (0.72); the launches traced: 423 us -> 307 us
  waiting for transfers between devices: 212 us -> 9.28 us
  Pallas kernels: 0 us -> 112 us
  matrix products: 55.1 us -> 33.1 us
  local copies, waits for them, and re-layouts: 96.4 us -> 90.6 us
    all_gather x4 -> x0, waiting for transfers between devices: 209 us -> none  [the longest x1 59.6 us: body(): lax.all_gather(w_query, ('sp', 'dp'), axis=0, tiled=True)]
    pallas_call x0 -> x1, Pallas kernels: none -> 112 us  [projected(): pl.pallas_call(functools.partial(project_kernel, grid), out_shape=(jax.Sh...]
    dot_general x4 -> x1, matrix products: 33.8 us -> 12.2 us  [body(): result = jnp.dot(retained, out_rows, preferred_element_type=jnp.float32)]
    pad x4, local copies, waits for them, and re-layouts: 37.1 us -> 24.2 us  [retain(): lax.associative_scan(combine_pairs, (carried, local_state), axis=1)]
    all_gather x1, waiting for transfers between devices: 0.01 us -> 9.26 us  [carried_in(): lax.all_gather(a.astype(kind), axis)]
    another operation x4, local copies, waits for them, and re-layouts: 8.35 us -> 13.5 us  [rotate(): paired = stacked.reshape(stacked.shape[0], stacked.shape[1], -1, 2)]
    unnamed x29 -> x32, local copies, waits for them, and re-layouts: 25.3 us -> 23.7 us
  transfers between devices with their start and end apart: 5 -> 1, of which waited for: 4 -> 1; matrix products, arithmetic and copies ran while one was open for 30% -> 14% of each run, Pallas kernels for 0% -> 0%
where the time goes in v1:
time: 308 us; the launch traced here: 307 us
  Pallas kernels  112 us (36%)
  local copies, waits for them, and re-layouts  90.6 us (29%)
  matrix products  33.1 us (11%)
  other arithmetic  28.3 us (9%)
  blocking collectives  19.4 us (6%)
  between operations  14.4 us (5%)
  waiting for transfers between devices  9.28 us (3%)
    pallas_call x1, Pallas kernels, projected(): pl.pallas_call(functools.partial(project_kernel, grid), out_shape=(jax.Sh...  112 us
    pad x4, local copies, waits for them, and re-layouts, retain(): lax.associative_scan(combine_pairs, (carried, local_state), axis=1)  24.2 us
    unnamed x32, local copies, waits for them, and re-layouts  23.7 us
    unnamed x1, blocking collectives  19.4 us
    another operation x4, local copies, waits for them, and re-layouts, rotate(): paired = stacked.reshape(stacked.shape[0], stacked.shape[1], -1, 2)  13.5 us
    dot_general x1, matrix products, body(): result = jnp.dot(retained, out_rows, preferred_element_type=jnp.float32)  12.2 us
    dot_general x1, matrix products, retain(): jnp.einsum('gncd,gnde->gnce', query_blocks.astype(jnp.float32) * from_sta...  11.1 us
    add x9, other arithmetic, combine_pairs(): later[0][..., None, None] * earlier[1] + later[1]  9.62 us
  transfers between devices with their start and end apart: 1, of which 1 were waited for; matrix products, arithmetic and copies ran while one was open for 14% of the time, Pallas kernels for 0%

profile of v1, /device:TPU:28, one launch (start us, length us, event | category | flops | bytes accessed | tf_op | source)
XLA Modules:
  0.0 307.3 jit_solution(15678449986919876944)
XLA Ops:
  7.5 2.1 pad_maximum_fusion.2.own_ref
  9.6 112.0 %shard_map.73 = (bf16[512,4096]{1,0:T(8,128)(2,1)}, bf16[2048,2048]{1,0:T(8,128)(2,1)}) custom-call(bf16[512,2048]{1,0:T(8,128)(2,1)} %bitcast.100, f32[1,2048]{1,0:T(1,128)} %bitcast.102, bf16[64,6144]{1,0:T(8,128)(2,1)} %pad_maximum_fusion.2.own_ref), custom_call_target="tpu_custom_call" | custom-call | tf_op jit(solution)/shard_map/pallas_call | solution.py:200
  121.6 3.3 %slice_bitcast_fusion = bf16[64,8,16,128]{3,1,2,0:T(8,128)(2,1)} fusion(bf16[512,4096]{1,0:T(8,128)(2,1)} %get-tuple-element.51), kind=kLoop, calls=%fused_computation.34 | loop fusion | bytes 4194304
  124.9 2.5 slice_convert_fusion.1
  127.6 2.2 copy.86
  129.8 3.6 %copy.52 = f32[512,1024]{0,1:T(8,128)} copy(f32[512,1024]{1,0:T(8,128)} %get-tuple-element.68) | data formatting | bytes 4194304 | tf_op jit(solution)/shard_map/reshape;reshape | solution.py:253
  133.4 3.5 %reshape.201 = f32[512,8,64,2]{0,3,2,1:T(2,128)} reshape(f32[512,1024]{0,1:T(8,128)} %copy.52) | data formatting | bytes 4194304 | tf_op jit(solution)/shard_map/reshape;reshape | solution.py:253
  136.9 2.9 copy.58
  139.8 3.5 %reshape.202 = f32[512,8,64,2]{0,3,2,1:T(2,128)} reshape(f32[512,1024]{0,1:T(8,128)} %copy.58) | data formatting | bytes 4194304 | tf_op jit(solution)/shard_map/reshape;reshape | solution.py:253
  143.8 8.2 %fusion.31 = (f32[512,8,64,1]{0,3,2,1:T(1,128)S(1)}, f32[512,8,64,1]{0,3,2,1:T(1,128)S(1)}, f32[512,8,64,1]{0,3,2,1:T(1,128)S(1)}, f32[512,8,64,1]{0,3,2,1:T(1,128)S(1)}) fusion(f32[512,8,64,2]{0,3,2,1:T(2,128)} %reshape.201, f32[512,8,64,2]{0,3,2,1:T(2,128)} %reshape.202), kind=kLoop, calls=%fused_computation.80 | loop fusion | bytes 8388608 | tf_op jit(solution)/shard_map/slice | solution.py:254
  152.0 1.8 subtract_convert_fusion
  155.8 1.9 copy.62
  158.8 3.2 %fusion.8 = f32[16,4,128,128]{3,2,1,0:T(8,128)S(1)} fusion(bf16[16,4,128,128]{3,0,2,1:T(8,128)(2,1)S(1)} %bitcast_bitcast_fusion, f32[16,4,128]{2,1,0:T(4,128)S(1)} %get-tuple-element.87, bf16[4,128,8,128]{3,1,0,2:T(8,128)(2,1)S(1)} %copy.62), kind=kOutput, calls=%fused_computation.21 | convolution fusion | flops 272629760 | bytes 7372800 | tf_op jit(solution)/shard_map/gncd,gnce->gnde/dot_general | solution.py:306
  162.3 1.6 copy-done.2
  165.4 11.8 %pad.119 = f32[16,3,128,128]{3,2,1,0:T(8,128)} pad(f32[16,2,128,128]{3,2,1,0:T(8,128)S(1)} %pad_add_fusion, f32[]{:T(128)} %constant.15.clone.1), padding=0_0_0x0_0_1x0_0_0x0_0_0 | pad | bytes 5242884
  177.2 2.1 add_convert_fusion
  179.4 12.1 %pad.31 = f32[16,4,128,128]{3,2,1,0:T(8,128)} pad(f32[16,2,128,128]{3,2,1,0:T(8,128)S(1)} %pad_add_fusion, f32[]{:T(128)} %constant.15.clone.1), padding=0_0_0x1_0_1x0_0_0x0_0_0 | pad | bytes 6291460 | tf_op jit(solution)/shard_map/pad | solution.py:310
  193.0 19.4 %all-reduce.10 = bf16[128]{0:T(256)(128)(2,1)S(1)} all-reduce(bf16[128]{0:T(256)(128)(2,1)S(1)} %dynamic-update-slice), channel_id=2, replica_groups=mesh['sp'=8,'dp'=4] {'sp'}, use_global_device_ids=true, to_apply=%add.10 | all-reduce | flops 128 | bytes 512
  213.9 1.5 copy.55
  215.5 2.5 convert_element_type.79
  218.0 2.7 copy.56
  220.6 2.7 copy.66
  223.4 2.1 fusion.30
  225.6 12.1 %pad.30 = f32[16,4,128,128]{3,2,1,0:T(8,128)} pad(f32[16,2,128,128]{3,2,1,0:T(8,128)S(1)} %pad_maximum_fusion, f32[]{:T(128)} %constant.15.clone.1), padding=0_0_0x0_1_1x0_0_0x0_0_0 | pad | bytes 6291460 | tf_op jit(solution)/shard_map/pad | solution.py:310
  237.9 5.2 %slice_add_fusion = f32[16,3,128,128]{3,2,1,0:T(8,128)} fusion(f32[16,4,128,128]{3,2,1,0:T(8,128)} %pad.31, f32[16,4,128,128]{3,2,1,0:T(8,128)} %pad.30), kind=kLoop, calls=%fused_computation.15 | loop fusion | flops 786432 | bytes 9437184 | tf_op jit(solution)/shard_map/add | solution.py:310
  243.1 9.3 %all-gather.4.cloned.1.call-done = bf16[128,1,128,128]{3,2,1,0:T(8,128)(2,1)} async-done(((bf16[16,1,128,128]{3,2,1,0:T(8,128)(2,1)}), bf16[128,1,128,128]{3,2,1,0:T(8,128)(2,1)}) %all-gather.4.cloned.1.call-update) | async-done | bytes 4194320 | tf_op jit(solution)/shard_map/all_gather | solution.py:227
  252.5 9.4 %while.12 = (s32[]{:T(128)}, f32[16,128,128]{2,1,0:T(8,128)S(1)}, s32[]{:T(128)}, bf16[8,16]{1,0:T(8,128)(2,1)S(1)}, bf16[8,16,128,128]{3,2,1,0:T(8,128)(2,1)}, /*index=5*/s32[]{:T(128)}, s32[]{:T(128)}, s32[]{:T(128)}) while((s32[]{:T(128)}, f32[16,128,128]{2,1,0:T(8,128)S(1)}, s32[]{:T(128)}, bf16[8,16]{1,0:T(8,128)(2,1)S(1)}, ...), condition=%wide.region_1.2_spmd, body=%wide.region_0.1_spmd.sunk | while | flops 786453 | bytes 2621735 | solution.py:241
  261.9 11.1 %fusion.1 = f32[16,4,128,128]{2,3,1,0:T(8,128)} fusion(f32[16,3,128,128]{3,2,1,0:T(8,128)} %slice_add_fusion, f32[16,128,128]{2,1,0:T(8,128)S(1)} %get-tuple-element.52, f32[16,4]{1,0:T(8,128)S(1)} %concatenate.44.clone, f32[16,4,128]{2,1,0:T(4,128)S(1)} %get-tuple-element.86, bf16[4,128,8,128]{3,1,0,2:T(8,128)(2,1)S(1)} %copy-done.10), kind=kOutput, calls=%fused_computation.7 | convolution fusion | flops 1615855616 | bytes 9470208 | tf_op jit(solution)/shard_map/gncd,gnde->gnce/dot_general | solution.py:316
  273.0 6.6 %fusion.28 = (f32[4,128,16]{1,0,2:T(4,128)S(1)}, f32[4,128,16]{1,0,2:T(4,128)S(1)}, f32[4,128,16,128]{1,3,0,2:T(8,128)}) fusion(f32[16,4,128,128]{2,3,1,0:T(8,128)} %fusion.1, bf16[4,128,16,128]{1,3,0,2:T(8,128)(2,1)} %copy.66, f32[128,128]{1,0:T(8,128)S(1)} %fusion.20, f32[16,4]{1,0:T(8,128)S(1)} %copy.65, pred[128,128]{1,0:T(8,128)(4,1)S(1)} %fusion.21, ...), kind=kOutput, calls=%fused_computation.77 | convolution fusion | flops 547340288 | bytes 12730624 | tf_op jit(solution)/shard_map/gncm,gnme->gnce/dot_general | solution.py:301
  280.0 5.5 %copy.73 = f32[4,128,16,128]{3,2,1,0:T(8,128)} copy(f32[4,128,16,128]{1,3,0,2:T(8,128)} %get-tuple-element.98) | data formatting | bytes 8388608 | tf_op jit(solution)/shard_map/add | solution.py:322
  286.7 1.6 copy-done.9
  288.2 12.2 %fusion.7 = bf16[1,512,2048]{2,1,0:T(8,128)(2,1)} fusion(bf16[2048,2048]{1,0:T(8,128)(2,1)} %get-tuple-element.53, f32[64,8,16,128]{3,2,1,0:T(8,128)S(1)} %bitcast.98, f32[64,8,16,128]{3,2,1,0:T(8,128)S(1)} %bitcast.99, f32[64,8,16,128]{3,2,1,0:T(8,128)S(1)} %bitcast.97), kind=kOutput, calls=%fused_computation.17 | convolution fusion | flops 4299161600 | bytes 23068672 | tf_op jit(solution)/shard_map/dot_general | solution.py:369
  (86 shorter events, 19.9 us)
Async XLA Ops:
  6.5 0.7 copy-start
  6.5 245.8 %all-gather.4.cloned.1.call-start = ((), (), s32[]{:S(2)}) async-start(), calls=%async_computation | async-start | bytes 4718592 | tf_op jit(solution)/shard_map/all_gather | solution.py:227
  121.6 3.3 %copy-start.6 = (bf16[512,4096]{1,0:T(8,128)(2,1)S(1)}, bf16[512,4096]{1,0:T(8,128)(2,1)}, u32[]{:S(2)}) copy-start(bf16[512,4096]{1,0:T(8,128)(2,1)} %get-tuple-element.51) | copy-start | bytes 12582916
  129.8 27.9 %copy-start.3 = (bf16[64,8,16,128]{3,2,1,0:T(8,128)(2,1)}, bf16[64,8,16,128]{3,2,1,0:T(8,128)(2,1)S(1)}, u32[]{:S(2)}) copy-start(bf16[64,8,16,128]{3,2,1,0:T(8,128)(2,1)S(1)} %copy.86) | copy-start | bytes 6291460
  157.7 1.0 copy-start.7
  162.0 1.9 copy-start.2
  164.1 1.0 copy-start.5
  179.4 12.2 %copy-start.11 = (u32[32]{0:T(128)S(1)}, u32[32]{0:T(128)}, u32[]{:S(2)}) copy-start(u32[32]{0:T(128)} %constant.80) | copy-start | bytes 388
  215.5 5.2 %copy-start.4 = (bf16[64,8,16,128]{3,2,1,0:T(8,128)(2,1)S(1)}, bf16[64,8,16,128]{3,2,1,0:T(8,128)(2,1)}, u32[]{:S(2)}) copy-start(bf16[64,8,16,128]{3,2,1,0:T(8,128)(2,1)} %copy-done.3) | copy-start | bytes 6291460
  252.5 9.5 %copy-start.10 = (bf16[4,128,8,128]{3,1,0,2:T(8,128)(2,1)S(1)}, bf16[4,128,8,128]{3,1,0,2:T(8,128)(2,1)}, u32[]{:S(2)}) copy-start(bf16[4,128,8,128]{3,1,0,2:T(8,128)(2,1)} %copy.56) | copy-start | bytes 3145732
  261.9 11.1 %copy-start.8 = (bf16[4,128,8,128]{3,1,0,2:T(8,128)(2,1)S(1)}, bf16[4,128,8,128]{3,1,0,2:T(8,128)(2,1)}, u32[]{:S(2)}) copy-start(bf16[4,128,8,128]{3,1,0,2:T(8,128)(2,1)} %copy-done.7) | copy-start | bytes 3145732
  286.0 2.2 copy-start.9
  288.2 12.2 %copy-start.1 = (f32[1,8,32]{2,1,0:T(8,128)S(1)}, f32[1,8,32]{2,1,0:T(8,128)}, u32[]{:S(2)}) copy-start(f32[1,8,32]{2,1,0:T(8,128)} %param.15) | copy-start | bytes 3076
Sparse Core Ops, SparseCore 0:
  179.5 72.8 all-gather.3

commit v2 on v1

--- a/solution.py
+++ b/solution.py
@@ -221,106 +221,200 @@
     )(token_rows, norm_gain[None, :], own_rows)
 
 
-def carried_in(x, axis, join, neutral):
-    place = lax.axis_index(axis)
-    gathered = jax.tree.map(
-        lambda a, kind: lax.all_gather(a.astype(kind), axis), x, (jnp.bfloat16, jnp.bfloat16)
-    )
-    state = jax.tree.map(lambda a, e: jnp.zeros_like(a) + jnp.asarray(e, a.dtype), x, neutral)
-
-    def one(lap, state):
-        return join(
-            state,
-            jax.tree.map(
-                lambda a, own: lax.dynamic_index_in_dim(a, lap, 0, False).astype(own.dtype),
-                gathered,
-                x,
-            ),
-        )
-
-    return lax.fori_loop(0, place, one, state)
-
-
 def rope_tables(length, head_depth, first_pos):
     half_depth = head_depth // 2
-    inverse = ROPE_BASE ** (-(jnp.arange(half_depth, dtype=jnp.float32) / (half_depth - 1)))
+    entry = jnp.arange(head_depth)
+    inverse = ROPE_BASE ** (-((entry // 2).astype(jnp.float32) / (half_depth - 1)))
     places = first_pos.astype(jnp.float32) + jnp.arange(length, dtype=jnp.float32)
     angles = places[:, None] * inverse[None, :]
-    return (jnp.cos(angles), jnp.sin(angles))
-
-
-def rotate(stacked, cosine_table, sine_table):
-    paired = stacked.reshape(stacked.shape[0], stacked.shape[1], -1, 2)
-    first_part = paired[..., 0]
-    second_part = paired[..., 1]
-    cos_rows = cosine_table[:, None, :]
-    sin_rows = sine_table[:, None, :]
-    turned = jnp.stack(
-        [
-            first_part * cos_rows - second_part * sin_rows,
-            second_part * cos_rows + first_part * sin_rows,
+    sign = jnp.where(entry % 2 == 0, -1.0, 1.0)
+    return (jnp.cos(angles), jnp.sin(angles) * sign)
+
+
+def retain_kernel(shards, proj_ref, cos_ref, sin_ref, rate_ref, kept_ref, key_ref, query_ref,
+                  before_ref, local_ref, inner_ref, sent_ref, came_ref, send_sem, recv_sem):
+    place = lax.axis_index("sp")
+    dp_at = lax.axis_index("dp")
+    count = proj_ref.shape[0]
+    blocks = count // BLOCK
+    value_at = HEADS * DK
+    half = HEADS * GROUP_W
+    query_at = value_at + 2 * half
+    first, last = place == 0, place == shards - 1
+
+    barrier = pltpu.get_barrier_semaphore()
+
+    @pl.when(jnp.logical_not(first))
+    def _():
+        pl.semaphore_signal(
+            barrier, inc=1, device_id={"sp": place - 1, "dp": dp_at}, device_id_type=MESH
+        )
+
+    @pl.when(jnp.logical_not(last))
+    def _():
+        pl.semaphore_signal(
+            barrier, inc=1, device_id={"sp": place + 1, "dp": dp_at}, device_id_type=MESH
+        )
+
+    pl.semaphore_wait(barrier, jnp.where(first, 0, 1) + jnp.where(last, 0, 1))
+
+    def columns(start, h):
+        return pl.ds(pl.multiple_of(start + h * DK, DK), DK)
+
+    def turned(start, h, n):
+        rows = pl.ds(n * BLOCK, BLOCK)
+        own = proj_ref[rows, columns(start, h)].astype(jnp.float32)
+        even = lax.rem(lax.broadcasted_iota(jnp.int32, own.shape, 1), 2) == 0
+        other = jnp.where(even, pltpu.roll(own, DK - 1, 1), pltpu.roll(own, 1, 1))
+        return own * cos_ref[rows, :] + other * sin_ref[rows, :]
+
+    def values(h, n):
+        rows = pl.ds(n * BLOCK, BLOCK)
+        return jnp.concatenate(
+            [proj_ref[rows, columns(value_at, h)], proj_ref[rows, columns(value_at + half, h)]],
+            axis=1,
+        )
+
+    def fade(total):
+        return jnp.exp(jnp.full((1, DV), -total * BLOCK, jnp.float32))
+
+    def hand_on(h):
+        return pltpu.make_async_remote_copy(
+            src_ref=sent_ref.at[h], dst_ref=came_ref.at[h],
+            send_sem=send_sem.at[h], recv_sem=recv_sem.at[h],
+            device_id={"sp": place + 1, "dp": dp_at}, device_id_type=MESH,
+        )
+
+    def local_part(h, _):
+        state = jnp.zeros((DK, DV), jnp.float32)
+        offset = lax.broadcasted_iota(jnp.int32, (BLOCK, DK), 0).astype(jnp.float32)
+        for n in range(blocks):
+            rate = rate_ref[h, n]
+            key_rot = (turned(0, h, n) * DK ** (-0.5)).astype(jnp.bfloat16)
+            key_ref[h, n] = key_rot
+            scaled = (
+                key_rot.astype(jnp.float32) * jnp.exp(-rate * (BLOCK - 1.0 - offset))
+            ).astype(jnp.bfloat16)
+            before_ref[h, n] = state
+            state = fade(rate) * state + lax.dot_general(
+                scaled, values(h, n), (((0,), (0,)), ((), ())),
+                preferred_element_type=jnp.float32,
+            )
+        local_ref[h] = state
+
+        @pl.when(first)
+        def _():
+            came_ref[h] = jnp.zeros((DK, DV), jnp.bfloat16)
+            sent_ref[h] = state.astype(jnp.bfloat16)
+            hand_on(h).start()
+        return 0
+
+    def inner_part(h, _):
+        shape = (BLOCK, BLOCK)
+        distance = (
+            lax.broadcasted_iota(jnp.int32, shape, 0) - lax.broadcasted_iota(jnp.int32, shape, 1)
+        ).astype(jnp.float32)
+        for n in range(blocks):
+            query_rot = turned(query_at, h, n).astype(jnp.bfloat16)
+            query_ref[h, n] = query_rot
+            scores = lax.dot_general(
+                query_rot, key_ref[h, n], (((1,), (1,)), ((), ())),
+                preferred_element_type=jnp.float32,
+            )
+            within = jnp.where(
+                distance >= 0.0, jnp.exp(-rate_ref[h, n] * jnp.maximum(distance, 0.0)), 0.0
+            )
+            inner_ref[h, n] = jnp.dot(
+                (scores * within).astype(jnp.bfloat16), values(h, n),
+                preferred_element_type=jnp.float32,
+            )
+        return 0
+
+    def chain_part(h, _):
+        total = rate_ref[h, 0]
+        for n in range(1, blocks):
+            total = total + rate_ref[h, n]
+        pltpu.make_async_copy(came_ref.at[h], came_ref.at[h], recv_sem.at[h]).wait()
+
+        @pl.when(jnp.logical_not(last))
+        def _():
+            sent_ref[h] = (
+                fade(total) * came_ref[h].astype(jnp.float32) + local_ref[h]
+            ).astype(jnp.bfloat16)
+            hand_on(h).start()
+        return 0
+
+    def finish_part(h, _):
+        incoming = came_ref[h].astype(jnp.float32)
+        offset = lax.broadcasted_iota(jnp.int32, (BLOCK, DV), 0).astype(jnp.float32)
+        total = jnp.float32(0.0)
+        for n in range(blocks):
+            rate = rate_ref[h, n]
+            before = before_ref[h, n] + fade(total) * incoming
+            cross = jnp.dot(
+                query_ref[h, n], before.astype(jnp.bfloat16), preferred_element_type=jnp.float32
+            )
+            mixed = inner_ref[h, n] + jnp.exp(-rate * (offset + 1.0)) * cross
+            mean = jnp.sum(mixed, axis=1, keepdims=True) / DV
+            square = jnp.sum(mixed * mixed, axis=1, keepdims=True) / DV
+            kept = (
+                (mixed - mean) * lax.rsqrt(square - mean * mean + EPS_GROUP)
+            ).astype(jnp.bfloat16)
+            rows = pl.ds(n * BLOCK, BLOCK)
+            kept_ref[rows, columns(0, h)] = kept[:, :GROUP_W]
+            kept_ref[rows, columns(half, h)] = kept[:, GROUP_W:]
+            total = total + rate
+        return 0
+
+    lax.fori_loop(0, HEADS, local_part, 0)
+    early = place < shards // 2
+
+    @pl.when(jnp.logical_not(early))
+    def _():
+        lax.fori_loop(0, HEADS, inner_part, 0)
+
+    @pl.when(jnp.logical_not(first))
+    def _():
+        lax.fori_loop(0, HEADS, chain_part, 0)
+
+    @pl.when(early)
+    def _():
+        lax.fori_loop(0, HEADS, inner_part, 0)
+
+    lax.fori_loop(0, HEADS, finish_part, 0)
+
+    @pl.when(jnp.logical_not(last))
+    def _():
+        def drain(h, _):
+            hand_on(h).wait_send()
+            return 0
+        lax.fori_loop(0, HEADS, drain, 0)
+
+
+def retained_rows(shards, proj, cosine, sine, own_rates):
+    count = proj.shape[0]
+    blocks = count // BLOCK
+    vmem = pl.BlockSpec(memory_space=pltpu.VMEM)
+    return pl.pallas_call(
+        functools.partial(retain_kernel, shards),
+        out_shape=jax.ShapeDtypeStruct((count, HEADS * DV), jnp.bfloat16),
+        in_specs=[vmem, vmem, vmem, pl.BlockSpec(memory_space=pltpu.SMEM)],
+        out_specs=vmem,
+        scratch_shapes=[
+            pltpu.VMEM((HEADS, blocks, BLOCK, DK), jnp.bfloat16),
+            pltpu.VMEM((HEADS, blocks, BLOCK, DK), jnp.bfloat16),
+            pltpu.VMEM((HEADS, blocks, DK, DV), jnp.float32),
+            pltpu.VMEM((HEADS, DK, DV), jnp.float32),
+            pltpu.VMEM((HEADS, blocks, BLOCK, DV), jnp.float32),
+            pltpu.VMEM((HEADS, DK, DV), jnp.bfloat16),
+            pltpu.VMEM((HEADS, DK, DV), jnp.bfloat16),
+            pltpu.SemaphoreType.DMA((HEADS,)),
+            pltpu.SemaphoreType.DMA((HEADS,)),
         ],
-        axis=-1,
-    )
-    return turned.reshape(stacked.shape)
-
-
-def combine_pairs(earlier, later):
-    return (earlier[0] * later[0], later[0][..., None, None] * earlier[1] + later[1])
-
-
-def from_earlier(last_decay, last_state):
-    _, incoming = carried_in(
-        (last_decay, last_state),
-        "sp",
-        combine_pairs,
-        (jnp.ones_like(last_decay), jnp.zeros_like(last_state)),
-    )
-    return incoming
-
-
-def retain(queries, keys_in, values_in, decay_rows, carry_in):
-    length, groups, head_depth = queries.shape
-    blocks = length // BLOCK
-
-    def by_block(stacked):
-        return stacked.reshape(blocks, BLOCK, groups, stacked.shape[-1]).transpose(2, 0, 1, 3)
-
-    query_blocks = by_block(queries)
-    key_blocks = by_block(keys_in)
-    value_blocks = by_block(values_in)
-    offsets = jnp.arange(BLOCK, dtype=jnp.float32)
-    distance = offsets[:, None] - offsets[None, :]
-    within = jnp.where(
-        distance >= 0.0, jnp.exp(-decay_rows[:, :, None, None] * jnp.maximum(distance, 0.0)), 0.0
-    )
-    scores = jnp.einsum(
-        "gncd,gnmd->gncm", query_blocks, key_blocks, preferred_element_type=jnp.float32
-    )
-    weighted = (scores * within).astype(jnp.bfloat16)
-    inner_sum = jnp.einsum(
-        "gncm,gnme->gnce", weighted, value_blocks, preferred_element_type=jnp.float32
-    )
-    to_end = jnp.exp(-decay_rows[:, :, None] * (BLOCK - 1.0 - offsets))
-    key_scaled = (key_blocks.astype(jnp.float32) * to_end[..., None]).astype(jnp.bfloat16)
-    local_state = jnp.einsum(
-        "gncd,gnce->gnde", key_scaled, value_blocks, preferred_element_type=jnp.float32
-    )
-    carried = jnp.exp(-decay_rows * BLOCK)
-    cum_decay, cum_state = lax.associative_scan(combine_pairs, (carried, local_state), axis=1)
-    incoming = carry_in(cum_decay[:, -1], cum_state[:, -1])
-    before_local = jnp.concatenate([jnp.zeros_like(cum_state[:, :1]), cum_state[:, :-1]], axis=1)
-    decay_before = jnp.concatenate([jnp.ones_like(cum_decay[:, :1]), cum_decay[:, :-1]], axis=1)
-    before = before_local + decay_before[..., None, None] * incoming[:, None]
-    from_start = jnp.exp(-decay_rows[:, :, None] * (offsets + 1.0))
-    cross_term = jnp.einsum(
-        "gncd,gnde->gnce",
-        query_blocks.astype(jnp.float32) * from_start[..., None],
-        before,
-        precision=lax.Precision.HIGHEST,
-    )
-    mixed = inner_sum + cross_term
-    return mixed.transpose(1, 2, 0, 3).reshape(length, groups, values_in.shape[-1])
+        compiler_params=pltpu.CompilerParams(
+            collective_id=1, has_side_effects=True, vmem_limit_bytes=40 * 1024 * 1024
+        ),
+    )(proj, cosine, sine, own_rates)
 
 
 def body(grid, tokens, norm_gain, w_query, w_key, w_value, w_out, decay_rate):
@@ -328,44 +422,11 @@
     local_count = token_rows.shape[0]
     own_rows = jnp.concatenate([w_key, w_value, w_query, w_out], axis=1)
     proj, out_rows = projected(grid, token_rows, norm_gain, own_rows)
-    key_end = w_key.shape[1]
-    value_end = key_end + w_value.shape[1]
-    key_sum = proj[:, :key_end]
-    value_sum = proj[:, key_end:value_end]
-    query_sum = proj[:, value_end:]
     shard_index = lax.axis_index("sp")
-    cosine_table, sine_table = rope_tables(local_count, DK, shard_index * local_count)
-    query_rot = rotate(
-        query_sum.astype(jnp.bfloat16).astype(jnp.float32).reshape(local_count, HEADS, DK),
-        cosine_table,
-        sine_table,
-    ).astype(jnp.bfloat16)
-    key_rot = (
-        rotate(
-            key_sum.astype(jnp.bfloat16).astype(jnp.float32).reshape(local_count, HEADS, DK),
-            cosine_table,
-            sine_table,
-        )
-        * DK ** (-0.5)
-    ).astype(jnp.bfloat16)
-    value_groups = value_sum.astype(jnp.bfloat16).reshape(local_count, 2 * HEADS, GROUP_W)
+    cosine, sine = rope_tables(local_count, DK, shard_index * local_count)
     blocks_here = local_count // BLOCK
     own_rates = lax.dynamic_slice_in_dim(decay_rate[0], shard_index * blocks_here, blocks_here, 1)
-    mixed = retain(
-        jnp.concatenate([query_rot, query_rot], axis=1),
-        jnp.concatenate([key_rot, key_rot], axis=1),
-        value_groups,
-        jnp.concatenate([own_rates, own_rates], axis=0),
-        from_earlier,
-    )
-    halves = mixed.reshape(local_count, 2, HEADS, GROUP_W)
-    mean_part = jnp.sum(halves, axis=(1, 3), keepdims=True) / DV
-    square_part = jnp.sum(halves * halves, axis=(1, 3), keepdims=True) / DV
-    retained = (
-        ((halves - mean_part) * lax.rsqrt(square_part - mean_part * mean_part + EPS_GROUP))
-        .astype(jnp.bfloat16)
-        .reshape(local_count, -1)
-    )
+    retained = retained_rows(grid[0] * grid[1], proj, cosine, sine, own_rates)
     result = jnp.dot(retained, out_rows, preferred_element_type=jnp.float32)
     return result.astype(jnp.bfloat16)[None]
 

time: 308 us -> 170 us (0.55)
  local copies, waits for them, and re-layouts: 90.6 us -> 2.91 us
  Pallas kernels: 112 us -> 155 us
  other arithmetic: 28.3 us -> 3.07 us
  matrix products: 33.1 us -> 9.11 us
  blocking collectives: 19.4 us -> 0 us
  between operations: 14.4 us -> 0.04 us
  waiting for transfers between devices: 9.28 us -> 0 us
    pallas_call x0 -> x1, Pallas kernels: none -> 42.7 us  [retained_rows(): pl.pallas_call(functools.partial(retain_kernel, shards), out_shape=jax.Sh...]
    pad x4 -> x0, local copies, waits for them, and re-layouts: 24.2 us -> none  [retain(): lax.associative_scan(combine_pairs, (carried, local_state), axis=1)]
    dot_general x3 -> x0, matrix products: 20.9 us -> none  [the longest x1 11.1 us: retain(): jnp.einsum('gncd,gnde->gnce', query_blocks.astype(jnp.float32) * from_sta...]
    unnamed x32 -> x4, local copies, waits for them, and re-layouts: 23.7 us -> 2.84 us
    unnamed x1 -> x0, blocking collectives: 19.4 us -> none
    another operation x6 -> x0, local copies, waits for them, and re-layouts: 17.7 us -> none  [the longest x4 13.5 us: rotate(): paired = stacked.reshape(stacked.shape[0], stacked.shape[1], -1, 2)]
    add x12 -> x0, other arithmetic: 15.1 us -> none  [the longest x9 9.62 us: combine_pairs(): later[0][..., None, None] * earlier[1] + later[1]]
    all_gather x1 -> x0, waiting for transfers between devices: 9.26 us -> none  [carried_in(): lax.all_gather(a.astype(kind), axis)]
  transfers between devices with their start and end apart: 1 -> 0, of which waited for: 1 -> 0; matrix products, arithmetic and copies ran while one was open for 14% -> 0% of each run, Pallas kernels for 0% -> 0%
where the time goes in v2:
time: 170 us
  Pallas kernels  155 us (91%)
  matrix products  9.11 us (5%)
  other arithmetic  3.07 us (2%)
  local copies, waits for them, and re-layouts  2.91 us (2%)
    pallas_call x1, Pallas kernels, projected(): pl.pallas_call(functools.partial(project_kernel, grid), out_shape=(jax.Sh...  112 us
    pallas_call x1, Pallas kernels, retained_rows(): pl.pallas_call(functools.partial(retain_kernel, shards), out_shape=jax.Sh...  42.7 us
    dot_general x1, matrix products, body(): result = jnp.dot(retained, out_rows, preferred_element_type=jnp.float32)  9.11 us

profile of v2, /device:TPU:28, one launch (start us, length us, event | category | flops | bytes accessed | tf_op | source)
XLA Modules:
  0.0 169.9 jit_solution(15898973449867855965)
XLA Ops:
  0.0 0.0 copy-start
  0.0 0.7 copy-done
  0.7 0.1 dynamic-slice_bitcast_fusion.rate_ref
  0.8 1.0 fusion.1
  1.8 2.1 %pad_maximum_fusion.own_ref = bf16[64,6144]{1,0:T(8,128)(2,1)} fusion(bf16[64,2048]{1,0:T(8,128)(2,1)} %param.12, bf16[64,1024]{1,0:T(8,128)(2,1)} %param.9, bf16[64,2048]{1,0:T(8,128)(2,1)} %param.11, bf16[64,1024]{1,0:T(8,128)(2,1)} %param.10), kind=kLoop, calls=%fused_computation.2 | loop fusion | flops 3145728 | bytes 1572864 | tf_op jit(solution)/shard_map/concatenate | solution.py:423
  3.8 112.1 %shard_map.73 = (bf16[512,4096]{1,0:T(8,128)(2,1)}, bf16[2048,2048]{1,0:T(8,128)(2,1)}) custom-call(bf16[512,2048]{1,0:T(8,128)(2,1)} %bitcast.8, f32[1,2048]{1,0:T(1,128)} %bitcast.9, bf16[64,6144]{1,0:T(8,128)(2,1)} %pad_maximum_fusion.own_ref), custom_call_target="tpu_custom_call" | custom-call | tf_op jit(solution)/shard_map/pallas_call | solution.py:200
  115.9 0.0 copy-start.1
  115.9 2.2 %copy-done.1 = bf16[512,4096]{1,0:T(8,128)(2,1)S(1)} copy-done((bf16[512,4096]{1,0:T(8,128)(2,1)S(1)}, bf16[512,4096]{1,0:T(8,128)(2,1)}, u32[]{:S(2)}) %copy-start.1) | copy-done | bytes 4194328
  118.1 42.7 %shard_map.74 = bf16[512,2048]{1,0:T(8,128)(2,1)S(1)} custom-call(bf16[512,4096]{1,0:T(8,128)(2,1)S(1)} %copy-done.1, f32[512,128]{1,0:T(8,128)S(1)} %get-tuple-element.10.cos_ref, f32[512,128]{1,0:T(8,128)S(1)} %get-tuple-element.9.sin_ref, f32[8,4]{1,0:T(8,128)S(1)} %dynamic-slice_bitcast_fusion.rate_ref), custom_call_target="tpu_custom_call" | custom-call | tf_op jit(solution)/shard_map/pallas_call | solution.py:398
  160.8 9.1 %fusion = bf16[1,512,2048]{2,1,0:T(8,128)(2,1)} fusion(bf16[512,2048]{1,0:T(8,128)(2,1)S(1)} %shard_map.74, bf16[2048,2048]{1,0:T(8,128)(2,1)} %get-tuple-element.8), kind=kOutput, calls=%fused_computation.1 | convolution fusion | flops 4296015872 | bytes 12582912 | tf_op jit(solution)/shard_map/dot_general | solution.py:430
  (2 shorter events, 0.0 us)
Async XLA Ops:
  0.0 0.7 copy-start
  115.9 2.2 %copy-start.1 = (bf16[512,4096]{1,0:T(8,128)(2,1)S(1)}, bf16[512,4096]{1,0:T(8,128)(2,1)}, u32[]{:S(2)}) copy-start(bf16[512,4096]{1,0:T(8,128)(2,1)} %get-tuple-element.7.proj_ref) | copy-start | bytes 12582916
